TPU v7x, 32 devices: a whole 2x2x4 slice. The times are simulated.
32 devices in a mesh: sp: 8 (over z, core), tp: 4 (over y, x).
Axes of the slice: x: 2, y: 2, z: 4, core: 2. Of those that a mesh axis runs over, the one named last changes fastest.
Arguments:
- queries: bfloat16 [2048, 1024], P('sp', 'tp'), may hold values from -250 to 250
- keys_values: bfloat16 [2, 2048, 256], P(None, 'sp'), may hold values from -8 to 8
- sink_logits: float32 [16], P('tp'), may hold values from 1 to 5
- proj_weight: bfloat16 [1024, 2048], P('tp'), may hold values from -0.75 to 0.75
- residual: bfloat16 [2048, 2048], P('sp', 'tp'), may hold values from -6 to 6
- norm_gain: float32 [2048], replicated, may hold values from 0.1 to 1.9
- routes: int32 [2048, 2], P('sp'), may hold values from 0 to 7, all different within a row; in each aligned block of 256 rows (0 to 255, 256 to 511, ...) at most 128 rows name the same one
- route_weights: float32 [2048, 2], P('sp'), may hold values from 0.2 to 1
- gate_weight: bfloat16 [8, 2048, 2048], P('sp', None, 'tp'), may hold values from -0.125 to 0.125
- up_weight: bfloat16 [8, 2048, 2048], P('sp', None, 'tp'), may hold values from -0.125 to 0.125
- down_weight: bfloat16 [8, 2048, 2048], P('sp', None, 'tp'), may hold values from -0.125 to 0.125
- shared_gate: bfloat16 [2048, 2048], P(None, 'tp'), may hold values from -0.125 to 0.125
- shared_up: bfloat16 [2048, 2048], P(None, 'tp'), may hold values from -0.125 to 0.125
- shared_down: bfloat16 [2048, 2048], P(None, 'tp'), may hold values from -0.125 to 0.125
Outputs:
- output: bfloat16 [2048, 2048], P('sp', 'tp')
Inputs may be any that keep to these rules, and one draw needn't show every extreme that they name: `routes`: the 2 experts of a position differ. In each aligned block of 256 positions no expert is named by more than 128 positions, and in some block one expert is named by exactly 128.
All inputs are finite; a program needn't handle non-finite values.
Results may differ from a plain program's by a relative error of at most 0.0067.
Values may be sent and summed in bfloat16 or wider, within the bound.
A program may use at most 64 MiB of HBM per device.

v0:
```python
import jax
import jax.numpy as jnp
from jax import lax
from jax.sharding import PartitionSpec as P

D = 2048
HEADS = 16
KV_HEADS = 4
HEAD_WIDTH = 64
WINDOW = 128
TOP_K = 2
EXP_DEV = 1
TOK_DEV = 256
norm_eps = 1e-06


def passed_along(value, axis, steps):
    count = lax.axis_size(axis)
    initial, last = (max(0, -steps), min(count, count - steps))
    return lax.ppermute(value, axis, [(source, source + steps) for source in range(initial, last)])


def per_device(
    queries,
    keys_values,
    sink_logits,
    proj_weight,
    residual,
    norm_gain,
    routes,
    route_weights,
    gate_weight,
    up_weight,
    down_weight,
    shared_gate,
    shared_up,
    shared_down,
):
    tp_index = lax.axis_index("tp")
    sp_index = lax.axis_index("sp")
    sp_count = lax.axis_size("sp")
    tp_count = lax.axis_size("tp")
    heads_here = sink_logits.shape[0]
    col_width = residual.shape[1]
    blocks = TOK_DEV // WINDOW
    kv_group = HEADS // KV_HEADS
    earlier_keys = passed_along(keys_values[:, TOK_DEV - WINDOW :, :], "sp", 1)
    extended = jnp.concatenate([earlier_keys, keys_values], axis=1)
    extended = extended.reshape(2, TOK_DEV + WINDOW, KV_HEADS, HEAD_WIDTH)
    head_ids = tp_index * heads_here + jnp.arange(heads_here, dtype=jnp.int32)
    chosen = jnp.take(extended, head_ids // kv_group, axis=2)
    earlier = chosen[:, :TOK_DEV].reshape(2, blocks, WINDOW, heads_here, HEAD_WIDTH)
    later = chosen[:, WINDOW:].reshape(2, blocks, WINDOW, heads_here, HEAD_WIDTH)
    banded = jnp.concatenate([earlier, later], axis=2)
    query_blocks = queries.reshape(blocks, WINDOW, heads_here, HEAD_WIDTH)
    score_matrix = jnp.einsum(
        "bqhd,bkhd->bhqk", query_blocks, banded[0], preferred_element_type=jnp.float32
    ) * HEAD_WIDTH ** (-0.5)
    query_pos = jnp.arange(WINDOW, dtype=jnp.int32)[:, None]
    key_pos = jnp.arange(2 * WINDOW, dtype=jnp.int32)[None, :]
    distance = WINDOW + query_pos - key_pos
    absolute = (
        sp_index * TOK_DEV
        + jnp.arange(blocks, dtype=jnp.int32)[:, None, None] * WINDOW
        - WINDOW
        + key_pos[None]
    )
    allowed = (distance >= 0)[None] & (distance < WINDOW)[None] & (absolute >= 0)
    masked = jnp.where(allowed[:, None], score_matrix, -jnp.inf)
    sink_value = sink_logits[None, :, None, None]
    highest = jnp.maximum(jnp.max(masked, axis=-1, keepdims=True), sink_value)
    weights_exp = jnp.exp(masked - highest)
    denominator = jnp.sum(weights_exp, axis=-1, keepdims=True) + jnp.exp(sink_value - highest)
    softmax_weights = (weights_exp / denominator).astype(jnp.bfloat16)
    attended_values = jnp.einsum(
        "bhqk,bkhd->bqhd", softmax_weights, banded[1], preferred_element_type=jnp.float32
    )
    attended_values = attended_values.astype(jnp.bfloat16).reshape(TOK_DEV, heads_here * HEAD_WIDTH)
    attended_all = lax.all_gather(attended_values, "tp", axis=1, tiled=True)
    weight_rows = proj_weight.shape[0]
    column_share = lax.all_to_all(
        proj_weight.reshape(weight_rows, tp_count, col_width),
        "tp",
        split_axis=1,
        concat_axis=0,
        tiled=True,
    )
    column_share = column_share.reshape(HEADS * HEAD_WIDTH, col_width)
    feature_sum = jnp.dot(attended_all, column_share, preferred_element_type=jnp.float32)
    stream_cols = (feature_sum + residual.astype(jnp.float32)).astype(jnp.bfloat16)
    stream_rows = lax.all_gather(stream_cols, "tp", axis=1, tiled=True)
    gate_eff = (norm_gain[None, :, None] * gate_weight.astype(jnp.float32)).astype(jnp.bfloat16)
    up_eff = (norm_gain[None, :, None] * up_weight.astype(jnp.float32)).astype(jnp.bfloat16)
    shared_gate_eff = (norm_gain[:, None] * shared_gate.astype(jnp.float32)).astype(jnp.bfloat16)
    shared_up_eff = (norm_gain[:, None] * shared_up.astype(jnp.float32)).astype(jnp.bfloat16)
    experts_total = EXP_DEV * sp_count
    capacity = 2 * TOK_DEV * TOP_K // experts_total
    rows_per_expert = sp_count * capacity
    flat_routes = routes.reshape(-1)
    onehot = (flat_routes[:, None] == jnp.arange(experts_total, dtype=jnp.int32)[None, :]).astype(
        jnp.int32
    )
    before = jnp.cumsum(onehot, axis=0) - onehot
    slot_rank = jnp.sum(before * onehot, axis=1)
    slot_index = (
        flat_routes % EXP_DEV * rows_per_expert + flat_routes // EXP_DEV * capacity + slot_rank
    )
    token_of = jnp.arange(TOK_DEV * TOP_K, dtype=jnp.int32) // TOP_K
    slot_owner = (
        jnp.full((EXP_DEV * rows_per_expert,), TOK_DEV, jnp.int32).at[slot_index].set(token_of)
    )
    picked_rows = jnp.take(stream_rows, slot_owner, axis=0, mode="fill", fill_value=0)
    arrived = lax.all_to_all(
        picked_rows.reshape(EXP_DEV, sp_count, capacity, stream_rows.shape[1]),
        "sp",
        split_axis=1,
        concat_axis=1,
        tiled=True,
    )
    arrived = arrived.reshape(EXP_DEV, rows_per_expert, D)
    routed_squares = jnp.sum(jnp.square(arrived.astype(jnp.float32)), axis=-1)
    gate_sum = jnp.einsum("erd,edf->erf", arrived, gate_eff, preferred_element_type=jnp.float32)
    up_sum = jnp.einsum("erd,edf->erf", arrived, up_eff, preferred_element_type=jnp.float32)
    own_squares = jnp.sum(jnp.square(stream_rows.astype(jnp.float32)), axis=-1)
    shared_gate_sum = jnp.dot(stream_rows, shared_gate_eff, preferred_element_type=jnp.float32)
    shared_up_sum = jnp.dot(stream_rows, shared_up_eff, preferred_element_type=jnp.float32)
    routed_scale = lax.rsqrt(routed_squares / D + norm_eps)[..., None]
    own_scale = lax.rsqrt(own_squares / D + norm_eps)[:, None]
    hidden = (jax.nn.silu(routed_scale * gate_sum) * (routed_scale * up_sum)).astype(jnp.bfloat16)
    shared_hidden = (jax.nn.silu(own_scale * shared_gate_sum) * (own_scale * shared_up_sum)).astype(
        jnp.bfloat16
    )
    routed_piece = lax.all_gather(hidden, "tp", axis=2, tiled=True)
    own_piece = lax.all_gather(shared_hidden[None], "tp", axis=2, tiled=True)
    expert_out = jnp.einsum(
        "erf,efd->erd", routed_piece, down_weight, preferred_element_type=jnp.float32
    )
    shared_out = jnp.dot(own_piece[0], shared_down, preferred_element_type=jnp.float32)
    outgoing = expert_out.astype(jnp.bfloat16).reshape(EXP_DEV, sp_count, capacity, col_width)
    returned = lax.all_to_all(outgoing, "sp", split_axis=1, concat_axis=1, tiled=True).reshape(
        EXP_DEV * rows_per_expert, col_width
    )
    picked = jnp.take(returned, slot_index, axis=0).reshape(TOK_DEV, TOP_K, col_width)
    routed_sum = jnp.einsum("nk,nkd->nd", route_weights, picked.astype(jnp.float32))
    return (stream_cols.astype(jnp.float32) + shared_out + routed_sum).astype(jnp.bfloat16)


def solution(mesh):
    placed = (
        P("sp", "tp"),
        P(None, "sp", None),
        P("tp"),
        P("tp", None),
        P("sp", "tp"),
        P(),
        P("sp", None),
        P("sp", None),
        P("sp", None, "tp"),
        P("sp", None, "tp"),
        P("sp", None, "tp"),
        P(None, "tp"),
        P(None, "tp"),
        P(None, "tp"),
    )
    return jax.shard_map(
        per_device, mesh=mesh, in_specs=placed, out_specs=P("sp", "tp"), check_vma=False
    )
```

profile of v0, /device:TPU:0, one launch (start us, length us, event | category | flops | bytes accessed | tf_op | source)
XLA Modules:
  0.0 293.3 jit_solution(9455327325811044780)
XLA Ops:
  6.5 1.2 copy.63
  7.8 3.2 %collective-permute-start = (bf16[2,128,256]{1,2,0:T(8,128)(2,1)S(1)}, bf16[2,128,256]{1,2,0:T(8,128)(2,1)}, u32[]{:S(2)}, u32[]{:S(2)}) collective-permute-start(bf16[2,128,256]{1,2,0:T(8,128)(2,1)S(1)} %slice.34), channel_id=1, source_target_pairs={{0,4},{4,8},{8,12},{12,16},{16,20},{20,24},{24,28},{1,5},{5,9},{9,... | collective-permute-start | bytes 393224 | tf_op jit(solution)/shard_map/ppermute | solution.py:20
  11.0 2.3 copy.73
  13.3 4.5 %all-to-all-start = ((bf16[256,4,512]{0,2,1:T(8,128)(2,1)}), bf16[256,4,512]{0,2,1:T(8,128)(2,1)S(1)}, u32[]{:S(2)}, u32[]{:S(2)}) async-start(bf16[256,4,512]{0,2,1:T(8,128)(2,1)} %bitcast.91), calls=%async_computation | async-start | bytes 2097152 | tf_op jit(solution)/shard_map/all_to_all | solution.py:81
  18.7 0.9 reshape.384
  19.6 1.0 pad_maximum_fusion
  20.7 1.4 gather_fusion
  22.0 1.1 select_bitcast_fusion
  24.0 1.0 reshape.382
  25.8 1.0 reshape.383
  27.6 1.5 fusion.48
  30.0 12.7 %all_gather.12 = bf16[256,1024]{0,1:T(8,128)(2,1)} all-gather(bf16[256,256]{0,1:T(8,128)(2,1)S(1)} %bitcast.95), channel_id=1, replica_groups=mesh['sp'=8,'tp'=4] {'tp'}, dimensions={1}, use_global_device_ids=true | all-gather | bytes 655360 | tf_op jit(solution)/shard_map/all_gather | solution.py:79
  42.7 1.3 copy.74
  44.0 2.6 fusion.25
  47.1 1.1 reduce-window.6
  48.9 2.4 scatter_custom_fusion
  51.4 20.4 %all-gather.6.cloned.1.call-done = bf16[256,2048]{1,0:T(8,128)(2,1)} async-done(((bf16[256,512]{1,0:T(8,128)(2,1)}), bf16[256,2048]{1,0:T(8,128)(2,1)}) %all-gather.6.cloned.1.call-update) | async-done | bytes 1048592 | tf_op jit(solution)/shard_map/all_gather | solution.py:91
  71.8 10.2 %gather_fusion.1 = bf16[1024,2048]{1,0:T(8,128)(2,1)} fusion(bf16[256,2048]{1,0:T(8,128)(2,1)} %all-gather.6.cloned.1.call-done, s32[1024]{0:T(1024)S(1)} %fusion.39), kind=kCustom, calls=%fused_computation.1 | custom fusion | bytes 8392704 | tf_op jit(solution)/shard_map/jit(_take)/gather | solution.py:112
  82.0 2.5 broadcast_select_fusion
  84.5 98.4 %all_to_all.25 = bf16[1,8,128,2048]{3,2,0,1:T(8,128)(2,1)S(1)} all-to-all(bf16[1,8,128,2048]{3,2,0,1:T(8,128)(2,1)S(1)} %broadcast_select_fusion), channel_id=1, replica_groups=mesh['sp'=8,'tp'=4] {'sp'}, dimensions={1} | all-to-all | bytes 8388608 | tf_op jit(solution)/shard_map/all_to_all | solution.py:113
  182.9 0.9 multiply_reduce_fusion
  184.5 2.4 fusion.3
  186.9 3.7 %multiply_convert_fusion.6 = bf16[1024,512]{1,0:T(8,128)(2,1)} fusion(f32[1024,512]{1,0:T(8,128)S(1)} %fusion.3, bf16[1024,2048]{1,0:T(8,128)(2,1)S(1)} %bitcast.89, bf16[1,2048,512]{2,1,0:T(8,128)(2,1)S(1)} %copy-done.11, f32[2048]{0:T(1024)S(1)} %copy-done.14, f32[1024]{0:T(1024)S(1)} %rsqrt_bitcast_fusion), kind=kOutput, calls=%fused_computation.18 | convolution fusion | flops 2154823680 | bytes 9449472 | tf_op jit(solution)/shard_map/erd,edf->erf/dot_general | solution.py:123
  191.0 50.3 %all-gather.10.cloned.1.call-done = bf16[1024,2048]{1,0:T(8,128)(2,1)} async-done(((bf16[1024,512]{1,0:T(8,128)(2,1)}), bf16[1024,2048]{1,0:T(8,128)(2,1)}) %all-gather.10.cloned.1.call-update) | async-done | bytes 4194320 | tf_op jit(solution)/shard_map/all_gather | solution.py:133
  241.3 5.5 %fusion.16 = bf16[1024,512]{1,0:T(8,128)(2,1)} fusion(bf16[1024,2048]{1,0:T(8,128)(2,1)} %all-gather.10.cloned.1.call-done, bf16[1,2048,512]{2,1,0:T(8,128)(2,1)S(1)} %copy-done), kind=kOutput, calls=%fused_computation.24 | convolution fusion | flops 2148007936 | bytes 7340032 | tf_op jit(solution)/shard_map/erf,efd->erd/dot_general | solution.py:135
  246.8 4.6 %all-to-all-start.2 = ((bf16[1,8,128,512]{3,2,0,1:T(8,128)(2,1)}), bf16[1,8,128,512]{3,2,0,1:T(8,128)(2,1)}, u32[]{:S(2)}, u32[]{:S(2)}) async-start(bf16[1,8,128,512]{3,2,0,1:T(8,128)(2,1)} %bitcast.93), calls=%async_computation.2 | async-start | bytes 2097152 | tf_op jit(solution)/shard_map/all_to_all | solution.py:140
  251.4 2.6 fusion.23
  254.0 1.6 fusion.27
  256.3 21.8 %all-to-all-done.2 = bf16[1,8,128,512]{3,2,0,1:T(8,128)(2,1)} async-done(((bf16[1,8,128,512]{3,2,0,1:T(8,128)(2,1)}), bf16[1,8,128,512]{3,2,0,1:T(8,128)(2,1)}, u32[]{:S(2)}, u32[]{:S(2)}) %all-to-all-start.2) | async-done | bytes 1048608 | tf_op jit(solution)/shard_map/all_to_all | solution.py:140
  278.0 3.3 %gather_fusion.2 = bf16[512,512]{1,0:T(8,128)(2,1)S(1)} fusion(bf16[1024,512]{1,0:T(8,128)(2,1)} %bitcast.25, s32[1024]{0:T(1024)S(1)} %pad_clamp_fusion), kind=kCustom, calls=%fused_computation.2 | custom fusion | bytes 1050624 | tf_op jit(solution)/shard_map/jit(_take)/gather | solution.py:143
  281.6 1.8 fusion.30
  283.4 3.4 %fusion.26 = bf16[256,512]{1,0:T(8,128)(2,1)} fusion(bf16[256,2048]{1,0:T(8,128)(2,1)} %all-gather.8.cloned.1.call-done, bf16[2048,512]{1,0:T(8,128)(2,1)} %param.27, f32[256,1,512]{2,1,0:T(1,128)} %fusion.30, bf16[256,512]{1,0:T(8,128)(2,1)S(1)} %copy-done.3), kind=kOutput, calls=%fused_computation.35 | convolution fusion | flops 537395200 | bytes 4194304 | tf_op jit(solution)/shard_map/dot_general | solution.py:138
  (82 shorter events, 7.2 us)
Async XLA Ops:
  6.5 234.7 %copy-start = (bf16[1,2048,512]{2,1,0:T(8,128)(2,1)S(1)}, bf16[1,2048,512]{2,1,0:T(8,128)(2,1)}, u32[]{:S(2)}) copy-start(bf16[1,2048,512]{2,1,0:T(8,128)(2,1)} %param.24) | copy-start | bytes 6291460
  7.8 5.5 %copy-start.2 = (bf16[2,256,256]{1,2,0:T(8,128)(2,1)}, bf16[2,256,256]{1,2,0:T(8,128)(2,1)S(1)}, u32[]{:S(2)}) copy-start(bf16[2,256,256]{1,2,0:T(8,128)(2,1)S(1)} %copy.63) | copy-start | bytes 786436
  7.8 10.9 %copy-start.4 = (bf16[256,256]{1,0:T(8,128)(2,1)S(1)}, bf16[256,256]{1,0:T(8,128)(2,1)}, u32[]{:S(2)}) copy-start(bf16[256,256]{1,0:T(8,128)(2,1)} %param.14) | copy-start | bytes 393220
  7.8 11.8 %collective-permute-start = (bf16[2,128,256]{1,2,0:T(8,128)(2,1)S(1)}, bf16[2,128,256]{1,2,0:T(8,128)(2,1)}, u32[]{:S(2)}, u32[]{:S(2)}) collective-permute-start(bf16[2,128,256]{1,2,0:T(8,128)(2,1)S(1)} %slice.34), channel_id=1, source_target_pairs={{0,4},{4,8},{8,12},{12,16},{16,20},{20,24},{24,28},{1,5},{5,9},{9,... | collective-permute-start | bytes 393224 | tf_op jit(solution)/shard_map/ppermute | solution.py:20
  13.3 29.4 %all-to-all-start = ((bf16[256,4,512]{0,2,1:T(8,128)(2,1)}), bf16[256,4,512]{0,2,1:T(8,128)(2,1)S(1)}, u32[]{:S(2)}, u32[]{:S(2)}) async-start(bf16[256,4,512]{0,2,1:T(8,128)(2,1)} %bitcast.91), calls=%async_computation | async-start | bytes 2097152 | tf_op jit(solution)/shard_map/all_to_all | solution.py:81
  17.8 54.0 %all-gather.6.cloned.1.call-start = ((), (), s32[]{:S(2)}) async-start(), calls=%async_computation.3 | async-start | bytes 1310720 | tf_op jit(solution)/shard_map/all_gather | solution.py:91
  22.0 5.6 %copy-start.6 = (pred[2,128,256]{1,2,0:T(8,128)(4,1)S(1)}, pred[2,128,256]{1,2,0:T(8,128)(4,1)}, u32[]{:S(2)}) copy-start(pred[2,128,256]{1,2,0:T(8,128)(4,1)} %broadcast_and_fusion) | copy-start | bytes 196612
  24.0 5.1 %copy-start.9 = (f32[4]{0:T(128)S(1)}, f32[4]{0:T(128)}, u32[]{:S(2)}) copy-start(f32[4]{0:T(128)} %param.16) | copy-start | bytes 52
  27.6 1.8 copy-start.5
  29.8 14.3 %copy-start.13 = (bf16[256,512]{1,0:T(8,128)(2,1)S(1)}, bf16[256,512]{1,0:T(8,128)(2,1)}, u32[]{:S(2)}) copy-start(bf16[256,512]{1,0:T(8,128)(2,1)} %param.18) | copy-start | bytes 786436
  42.7 4.0 %copy-start.7 = (s32[256,2]{0,1:T(2,128)S(1)}, s32[256,2]{0,1:T(2,128)}, u32[]{:S(2)}) copy-start(s32[256,2]{0,1:T(2,128)} %param.20) | copy-start | bytes 6148
  46.6 194.7 %all-gather.10.cloned.1.call-start = ((), (), s32[]{:S(2)}) async-start(), calls=%async_computation.5 | async-start | bytes 5242880 | tf_op jit(solution)/shard_map/all_gather | solution.py:133
  182.9 1.6 copy-start.10
  182.9 1.6 copy-start.14
  184.5 2.4 copy-start.11
  186.9 3.8 %copy-start.1 = (bf16[256,2048]{1,0:T(8,128)(2,1)S(1)}, bf16[256,2048]{1,0:T(8,128)(2,1)}, u32[]{:S(2)}) copy-start(bf16[256,2048]{1,0:T(8,128)(2,1)} %all-gather.6.cloned.1.call-done) | copy-start | bytes 3145732
  246.8 31.3 %all-to-all-start.2 = ((bf16[1,8,128,512]{3,2,0,1:T(8,128)(2,1)}), bf16[1,8,128,512]{3,2,0,1:T(8,128)(2,1)}, u32[]{:S(2)}, u32[]{:S(2)}) async-start(bf16[1,8,128,512]{3,2,0,1:T(8,128)(2,1)} %bitcast.93), calls=%async_computation.2 | async-start | bytes 2097152 | tf_op jit(solution)/shard_map/all_to_all | solution.py:140
  251.4 32.0 %all-gather.8.cloned.1.call-start = ((), (), s32[]{:S(2)}) async-start(), calls=%async_computation.4 | async-start | bytes 1310720 | tf_op jit(solution)/shard_map/all_gather | solution.py:134
  251.4 2.6 copy-start.12
  254.0 2.1 copy-start.8
  281.6 1.8 copy-start.3
Sparse Core Ops, SparseCore 0:
  46.7 25.0 all-gather.5
  190.8 50.3 all-gather.9
  255.8 26.7 all-gather.7
where the time goes:
time: 294 us; the launch traced here: 293 us
  blocking collectives  111 us (38%)
  waiting for transfers between devices  92.4 us (31%)
  local copies, waits for them, and re-layouts  30.1 us (10%)
  matrix products  25.3 us (9%)
  between operations  13.5 us (5%)
  starting transfers between devices  12.4 us (4%)
  other arithmetic  8.46 us (3%)
    all_to_all x1, blocking collectives, per_device(): lax.all_to_all(picked_rows.reshape(EXP_DEV, sp_count, capacity, stream_ro...  98.4 us
    all_gather x1, waiting for transfers between devices, per_device(): routed_piece = lax.all_gather(hidden, 'tp', axis=2, tiled=True)  50.3 us
    all_to_all x1, waiting for transfers between devices, per_device(): lax.all_to_all(outgoing, 'sp', split_axis=1, concat_axis=1, tiled=True)  21.8 us
    all_gather x1, waiting for transfers between devices, per_device(): stream_rows = lax.all_gather(stream_cols, 'tp', axis=1, tiled=True)  20.4 us
    all_gather x1, blocking collectives, per_device(): attended_all = lax.all_gather(attended_values, 'tp', axis=1, tiled=True)  12.7 us
    gather x1, local copies, waits for them, and re-layouts, per_device(): jnp.take(stream_rows, slot_owner, axis=0, mode='fill', fill_value=0)  10.2 us
  transfers between devices with their start and end apart: 6, of which 3 were waited for; matrix products, arithmetic and copies ran while one was open for 10% of the time, Pallas kernels for 0%

commit v1 on v0

--- a/solution.py
+++ b/solution.py
@@ -12,6 +12,18 @@
 EXP_DEV = 1
 TOK_DEV = 256
 norm_eps = 1e-06
+
+
+def summed_around(value, axis, dim, product):
+    size, place, rows = (lax.axis_size(axis), lax.axis_index(axis), value.shape[dim])
+    right = [(i, (i + 1) % size) for i in range(size)]
+    held, running = (value, None)
+    for step in range(size):
+        coming = lax.ppermute(held, axis, right) if step < size - 1 else None
+        take_in = product(held, (place - step) % size * rows)
+        running = take_in if running is None else running + take_in
+        held = coming
+    return running
 
 
 def passed_along(value, axis, steps):
@@ -130,10 +142,17 @@
     shared_hidden = (jax.nn.silu(own_scale * shared_gate_sum) * (own_scale * shared_up_sum)).astype(
         jnp.bfloat16
     )
-    routed_piece = lax.all_gather(hidden, "tp", axis=2, tiled=True)
     own_piece = lax.all_gather(shared_hidden[None], "tp", axis=2, tiled=True)
-    expert_out = jnp.einsum(
-        "erf,efd->erd", routed_piece, down_weight, preferred_element_type=jnp.float32
+    expert_out = summed_around(
+        hidden,
+        "tp",
+        2,
+        lambda shard, start: jnp.einsum(
+            "erf,efd->erd",
+            shard,
+            lax.dynamic_slice_in_dim(down_weight, start, shard.shape[2], axis=1),
+            preferred_element_type=jnp.float32,
+        ),
     )
     shared_out = jnp.dot(own_piece[0], shared_down, preferred_element_type=jnp.float32)
     outgoing = expert_out.astype(jnp.bfloat16).reshape(EXP_DEV, sp_count, capacity, col_width)

time: 294 us -> 314 us (1.068)
  waiting for transfers between devices: 92.4 us -> 108 us
    ppermute x0 -> x3, waiting for transfers between devices: none -> 66.2 us  [summed_around(): coming = lax.ppermute(held, axis, right) if step < size - 1 else None]
    all_gather x1 -> x0, waiting for transfers between devices: 50.3 us -> none  [per_device(): routed_piece = lax.all_gather(hidden, 'tp', axis=2, tiled=True)]
    dot_general x1 -> x4, matrix products: 5.49 us -> 7.51 us  [per_device(): jnp.einsum('erf,efd->erd', shard, lax.dynamic_slice_in_dim(down_weight, s...]
    unnamed x36 -> x38, local copies, waits for them, and re-layouts: 5.35 us -> 6.35 us
  transfers between devices with their start and end apart: 6 -> 8, of which waited for: 3 -> 5; matrix products, arithmetic and copies ran while one was open for 10% -> 11% of each run, Pallas kernels for 0% -> 0%
where the time goes in v1:
time: 314 us; the launch traced here: 313 us
  blocking collectives  111 us (35%)
  waiting for transfers between devices  108 us (34%)
  local copies, waits for them, and re-layouts  31.1 us (10%)
  matrix products  26.3 us (8%)
  starting transfers between devices  14.2 us (5%)
  between operations  13.8 us (4%)
  other arithmetic  8.48 us (3%)
    all_to_all x1, blocking collectives, per_device(): lax.all_to_all(picked_rows.reshape(EXP_DEV, sp_count, capacity, stream_ro...  98.4 us
    ppermute x3, waiting for transfers between devices, summed_around(): coming = lax.ppermute(held, axis, right) if step < size - 1 else None  66.2 us
    all_to_all x1, waiting for transfers between devices, per_device(): lax.all_to_all(outgoing, 'sp', split_axis=1, concat_axis=1, tiled=True)  21.8 us
    all_gather x1, waiting for transfers between devices, per_device(): stream_rows = lax.all_gather(stream_cols, 'tp', axis=1, tiled=True)  20.4 us
    all_gather x1, blocking collectives, per_device(): attended_all = lax.all_gather(attended_values, 'tp', axis=1, tiled=True)  12.8 us
    gather x1, local copies, waits for them, and re-layouts, per_device(): jnp.take(stream_rows, slot_owner, axis=0, mode='fill', fill_value=0)  10.2 us
    dot_general x4, matrix products, per_device(): jnp.einsum('erf,efd->erd', shard, lax.dynamic_slice_in_dim(down_weight, s...  7.51 us
    unnamed x38, local copies, waits for them, and re-layouts  6.35 us
  transfers between devices with their start and end apart: 8, of which 5 were waited for; matrix products, arithmetic and copies ran while one was open for 11% of the time, Pallas kernels for 0%

profile of v1, /device:TPU:0, one launch (start us, length us, event | category | flops | bytes accessed | tf_op | source)
XLA Modules:
  0.0 313.3 jit_solution(9047739267193468589)
XLA Ops:
  6.5 1.2 copy.63
  7.8 3.2 %collective-permute-start = (bf16[2,128,256]{1,2,0:T(8,128)(2,1)S(1)}, bf16[2,128,256]{1,2,0:T(8,128)(2,1)}, u32[]{:S(2)}, u32[]{:S(2)}) collective-permute-start(bf16[2,128,256]{1,2,0:T(8,128)(2,1)S(1)} %slice.34), channel_id=1, source_target_pairs={{0,4},{4,8},{8,12},{12,16},{16,20},{20,24},{24,28},{1,5},{5,9},{9,... | collective-permute-start | bytes 393224 | tf_op jit(solution)/shard_map/ppermute | solution.py:32
  11.0 2.3 copy.73
  13.3 4.5 %all-to-all-start = ((bf16[256,4,512]{0,2,1:T(8,128)(2,1)}), bf16[256,4,512]{0,2,1:T(8,128)(2,1)S(1)}, u32[]{:S(2)}, u32[]{:S(2)}) async-start(bf16[256,4,512]{0,2,1:T(8,128)(2,1)} %bitcast.109), calls=%async_computation | async-start | bytes 2097152 | tf_op jit(solution)/shard_map/all_to_all | solution.py:93
  20.7 1.4 gather_fusion
  27.7 1.5 fusion.61
  30.0 12.8 %all_gather.9 = bf16[256,1024]{0,1:T(8,128)(2,1)} all-gather(bf16[256,256]{0,1:T(8,128)(2,1)S(1)} %bitcast.113), channel_id=1, replica_groups=mesh['sp'=8,'tp'=4] {'tp'}, dimensions={1}, use_global_device_ids=true | all-gather | bytes 655360 | tf_op jit(solution)/shard_map/all_gather | solution.py:91
  42.8 1.3 copy.74
  44.1 2.6 fusion.20
  47.1 1.1 reduce-window.6
  48.9 2.4 scatter_custom_fusion
  51.4 20.4 %all-gather.4.cloned.1.call-done = bf16[256,2048]{1,0:T(8,128)(2,1)} async-done(((bf16[256,512]{1,0:T(8,128)(2,1)}), bf16[256,2048]{1,0:T(8,128)(2,1)}) %all-gather.4.cloned.1.call-update) | async-done | bytes 1048592 | tf_op jit(solution)/shard_map/all_gather | solution.py:103
  71.8 10.2 %gather_fusion.1 = bf16[1024,2048]{1,0:T(8,128)(2,1)} fusion(bf16[256,2048]{1,0:T(8,128)(2,1)} %all-gather.4.cloned.1.call-done, s32[1024]{0:T(1024)S(1)} %fusion.48), kind=kCustom, calls=%fused_computation.1 | custom fusion | bytes 8392704 | tf_op jit(solution)/shard_map/jit(_take)/gather | solution.py:124
  81.9 2.5 broadcast_select_fusion
  84.5 98.4 %all_to_all.25 = bf16[1,8,128,2048]{3,2,0,1:T(8,128)(2,1)S(1)} all-to-all(bf16[1,8,128,2048]{3,2,0,1:T(8,128)(2,1)S(1)} %broadcast_select_fusion), channel_id=1, replica_groups=mesh['sp'=8,'tp'=4] {'sp'}, dimensions={1} | all-to-all | bytes 8388608 | tf_op jit(solution)/shard_map/all_to_all | solution.py:125
  184.5 2.4 fusion.3
  186.9 2.7 multiply_convert_fusion.6
  190.7 1.5 collective-permute-start.1
  192.1 24.1 %collective-permute-done.1 = bf16[1,1024,512]{2,1,0:T(8,128)(2,1)} collective-permute-done((bf16[1,1024,512]{2,1,0:T(8,128)(2,1)S(1)}, bf16[1,1024,512]{2,1,0:T(8,128)(2,1)}, u32[]{:S(2)}, u32[]{:S(2)}) %collective-permute-start.1) | collective-permute-done | bytes 1048608 | tf_op jit(solution)/shard_map/ppermute | solution.py:22
  217.1 24.0 %collective-permute-done.2 = bf16[1,1024,512]{2,1,0:T(8,128)(2,1)} collective-permute-done((bf16[1,1024,512]{2,1,0:T(8,128)(2,1)}, bf16[1,1024,512]{2,1,0:T(8,128)(2,1)}, u32[]{:S(2)}, u32[]{:S(2)}) %collective-permute-start.2) | collective-permute-done | bytes 1048608 | tf_op jit(solution)/shard_map/ppermute | solution.py:22
  241.1 1.9 fusion.33
  243.0 1.9 fusion.27
  245.0 1.9 fusion.25
  246.9 18.1 %collective-permute-done.3 = bf16[1,1024,512]{2,1,0:T(8,128)(2,1)S(1)} collective-permute-done((bf16[1,1024,512]{2,1,0:T(8,128)(2,1)}, bf16[1,1024,512]{2,1,0:T(8,128)(2,1)S(1)}, u32[]{:S(2)}, u32[]{:S(2)}) %collective-permute-start.3) | collective-permute-done | bytes 1048608 | tf_op jit(solution)/shard_map/ppermute | solution.py:22
  265.0 1.7 add_convert_fusion
  266.7 4.3 %all-to-all-start.2 = ((bf16[1,8,128,512]{3,2,0,1:T(8,128)(2,1)}), bf16[1,8,128,512]{3,2,0,1:T(8,128)(2,1)}, u32[]{:S(2)}, u32[]{:S(2)}) async-start(bf16[1,8,128,512]{3,2,0,1:T(8,128)(2,1)} %bitcast.107), calls=%async_computation.2 | async-start | bytes 2097152 | tf_op jit(solution)/shard_map/all_to_all | solution.py:159
  271.2 2.6 fusion.18
  273.8 1.6 fusion.22
  276.0 21.8 %all-to-all-done.2 = bf16[1,8,128,512]{3,2,0,1:T(8,128)(2,1)} async-done(((bf16[1,8,128,512]{3,2,0,1:T(8,128)(2,1)}), bf16[1,8,128,512]{3,2,0,1:T(8,128)(2,1)}, u32[]{:S(2)}, u32[]{:S(2)}) %all-to-all-start.2) | async-done | bytes 1048608 | tf_op jit(solution)/shard_map/all_to_all | solution.py:159
  297.8 3.3 %gather_fusion.2 = bf16[512,512]{1,0:T(8,128)(2,1)S(1)} fusion(bf16[1024,512]{1,0:T(8,128)(2,1)} %bitcast.32, s32[1024]{0:T(1024)S(1)} %pad_clamp_fusion), kind=kCustom, calls=%fused_computation.2 | custom fusion | bytes 1050624 | tf_op jit(solution)/shard_map/jit(_take)/gather | solution.py:162
  301.3 1.8 fusion.39
  303.1 3.4 %fusion.21 = bf16[256,512]{1,0:T(8,128)(2,1)} fusion(bf16[256,2048]{1,0:T(8,128)(2,1)} %all-gather.6.cloned.1.call-done, bf16[2048,512]{1,0:T(8,128)(2,1)} %param.27, f32[256,1,512]{2,1,0:T(1,128)} %fusion.39, bf16[256,512]{1,0:T(8,128)(2,1)S(1)} %copy-done.4), kind=kOutput, calls=%fused_computation.33 | convolution fusion | flops 537395200 | bytes 4194304 | tf_op jit(solution)/shard_map/dot_general | solution.py:157
  (90 shorter events, 14.7 us)
Async XLA Ops:
  6.5 234.6 %copy-start = (bf16[1,2048,512]{2,1,0:T(8,128)(2,1)S(1)}, bf16[1,2048,512]{2,1,0:T(8,128)(2,1)}, u32[]{:S(2)}) copy-start(bf16[1,2048,512]{2,1,0:T(8,128)(2,1)} %param.24) | copy-start | bytes 6291460
  7.8 5.5 %copy-start.3 = (bf16[2,256,256]{1,2,0:T(8,128)(2,1)}, bf16[2,256,256]{1,2,0:T(8,128)(2,1)S(1)}, u32[]{:S(2)}) copy-start(bf16[2,256,256]{1,2,0:T(8,128)(2,1)S(1)} %copy.63) | copy-start | bytes 786436
  7.8 11.0 %copy-start.5 = (bf16[256,256]{1,0:T(8,128)(2,1)S(1)}, bf16[256,256]{1,0:T(8,128)(2,1)}, u32[]{:S(2)}) copy-start(bf16[256,256]{1,0:T(8,128)(2,1)} %param.14) | copy-start | bytes 393220
  7.8 11.8 %collective-permute-start = (bf16[2,128,256]{1,2,0:T(8,128)(2,1)S(1)}, bf16[2,128,256]{1,2,0:T(8,128)(2,1)}, u32[]{:S(2)}, u32[]{:S(2)}) collective-permute-start(bf16[2,128,256]{1,2,0:T(8,128)(2,1)S(1)} %slice.34), channel_id=1, source_target_pairs={{0,4},{4,8},{8,12},{12,16},{16,20},{20,24},{24,28},{1,5},{5,9},{9,... | collective-permute-start | bytes 393224 | tf_op jit(solution)/shard_map/ppermute | solution.py:32
  13.3 29.5 %all-to-all-start = ((bf16[256,4,512]{0,2,1:T(8,128)(2,1)}), bf16[256,4,512]{0,2,1:T(8,128)(2,1)S(1)}, u32[]{:S(2)}, u32[]{:S(2)}) async-start(bf16[256,4,512]{0,2,1:T(8,128)(2,1)} %bitcast.109), calls=%async_computation | async-start | bytes 2097152 | tf_op jit(solution)/shard_map/all_to_all | solution.py:93
  17.8 54.0 %all-gather.4.cloned.1.call-start = ((), (), s32[]{:S(2)}) async-start(), calls=%async_computation.3 | async-start | bytes 1310720 | tf_op jit(solution)/shard_map/all_gather | solution.py:103
  22.0 5.6 %copy-start.7 = (pred[2,128,256]{1,2,0:T(8,128)(4,1)S(1)}, pred[2,128,256]{1,2,0:T(8,128)(4,1)}, u32[]{:S(2)}) copy-start(pred[2,128,256]{1,2,0:T(8,128)(4,1)} %broadcast_and_fusion) | copy-start | bytes 196612
  24.1 5.1 %copy-start.10 = (f32[4]{0:T(128)S(1)}, f32[4]{0:T(128)}, u32[]{:S(2)}) copy-start(f32[4]{0:T(128)} %param.16) | copy-start | bytes 52
  27.7 1.8 copy-start.6
  29.8 14.3 %copy-start.14 = (bf16[256,512]{1,0:T(8,128)(2,1)S(1)}, bf16[256,512]{1,0:T(8,128)(2,1)}, u32[]{:S(2)}) copy-start(bf16[256,512]{1,0:T(8,128)(2,1)} %param.18) | copy-start | bytes 786436
  42.7 3.9 %copy-start.8 = (s32[256,2]{0,1:T(2,128)S(1)}, s32[256,2]{0,1:T(2,128)}, u32[]{:S(2)}) copy-start(s32[256,2]{0,1:T(2,128)} %param.20) | copy-start | bytes 6148
  182.9 1.6 copy-start.11
  182.9 1.6 copy-start.15
  184.5 2.4 copy-start.12
  186.9 29.9 %copy-start.1 = (bf16[256,2048]{1,0:T(8,128)(2,1)S(1)}, bf16[256,2048]{1,0:T(8,128)(2,1)}, u32[]{:S(2)}) copy-start(bf16[256,2048]{1,0:T(8,128)(2,1)} %all-gather.4.cloned.1.call-done) | copy-start | bytes 3145732
  189.7 1.0 copy-start.2
  190.7 25.5 %collective-permute-start.1 = (bf16[1,1024,512]{2,1,0:T(8,128)(2,1)S(1)}, bf16[1,1024,512]{2,1,0:T(8,128)(2,1)}, u32[]{:S(2)}, u32[]{:S(2)}) collective-permute-start(bf16[1,1024,512]{2,1,0:T(8,128)(2,1)S(1)} %bitcast.111), channel_id=1, source_target_pairs={{0,1},{1,2},{2,3},{3,0},{4,5},{5,6},{6,7},{7,4},{8,9},{9,10},{10,1... | collective-permute-start | bytes 3145736 | tf_op jit(solution)/shard_map/ppermute | solution.py:22
  216.2 24.9 %collective-permute-start.2 = (bf16[1,1024,512]{2,1,0:T(8,128)(2,1)}, bf16[1,1024,512]{2,1,0:T(8,128)(2,1)}, u32[]{:S(2)}, u32[]{:S(2)}) collective-permute-start(bf16[1,1024,512]{2,1,0:T(8,128)(2,1)} %collective-permute-done.1), channel_id=1, source_target_pairs={{0,1},{1,2},{2,3},{3,0},{4,5},{5,6},{6,7},{7,4},{8,9},{9,10},{10,1... | collective-permute-start | bytes 3145736 | tf_op jit(solution)/shard_map/ppermute | solution.py:22
  241.1 23.9 %collective-permute-start.3 = (bf16[1,1024,512]{2,1,0:T(8,128)(2,1)}, bf16[1,1024,512]{2,1,0:T(8,128)(2,1)S(1)}, u32[]{:S(2)}, u32[]{:S(2)}) collective-permute-start(bf16[1,1024,512]{2,1,0:T(8,128)(2,1)} %collective-permute-done.2), channel_id=1, source_target_pairs={{0,1},{1,2},{2,3},{3,0},{4,5},{5,6},{6,7},{7,4},{8,9},{9,10},{10,1... | collective-permute-start | bytes 3145736 | tf_op jit(solution)/shard_map/ppermute | solution.py:22
  266.7 31.0 %all-to-all-start.2 = ((bf16[1,8,128,512]{3,2,0,1:T(8,128)(2,1)}), bf16[1,8,128,512]{3,2,0,1:T(8,128)(2,1)}, u32[]{:S(2)}, u32[]{:S(2)}) async-start(bf16[1,8,128,512]{3,2,0,1:T(8,128)(2,1)} %bitcast.107), calls=%async_computation.2 | async-start | bytes 2097152 | tf_op jit(solution)/shard_map/all_to_all | solution.py:159
  271.1 32.0 %all-gather.6.cloned.1.call-start = ((), (), s32[]{:S(2)}) async-start(), calls=%async_computation.4 | async-start | bytes 1310720 | tf_op jit(solution)/shard_map/all_gather | solution.py:145
  271.1 2.6 copy-start.13
  273.7 2.1 copy-start.9
  301.3 1.8 copy-start.4
Sparse Core Ops, SparseCore 0:
  46.8 24.9 all-gather.3
  275.5 26.7 all-gather.5
